TPU v7x, 512 devices: a 8x2x16 block of a 8x16x16 slice. The times are simulated.
512 devices in a mesh: grp: 2 (over y), sp: 16 (over z), tp: 16 (over x, core).
Axes of the slice: x: 8, y: 2, z: 16, core: 2. Of those that a mesh axis runs over, the one named last changes fastest.
The devices are a block of a 8x16x16 slice.
Arguments:
- target: bfloat16 [4096, 2048], P(('grp', 'sp', 'tp')), parts along dimension 0, may hold values from -60 to 60
- source: bfloat16 [32768, 2048], P(('grp', 'sp', 'tp')), parts along dimension 0, may hold values from -120 to 120
- w_query: bfloat16 [2, 2048, 2048], P(None, None, 'tp'), may hold values from -0.176776695 to 0.176776695
- w_key: bfloat16 [2, 2048, 2048], P(None, None, 'tp'), may hold values from -0.176776695 to 0.176776695
- w_value: bfloat16 [2, 2048, 2048], P(None, None, 'tp'), may hold values from -0.125 to 0.125
- w_out: bfloat16 [2, 2048, 2048], P(None, 'tp'), may hold values from -0.125 to 0.125
- gains: float32 [2, 2, 2048], replicated, may hold values from 0.1 to 1.9
Outputs:
- mixed: bfloat16 [4096, 2048], P(('grp', 'sp', 'tp')), parts along dimension 0
There are 2 independent parts, one for each index of `grp`. A program takes and returns all parts, laid end to end along the dimension named above; an argument that names none is the same for every part. Nothing has to cross between parts.
All inputs are finite; a program needn't handle non-finite values.
Results may differ from a plain program's by a relative error of at most 0.025.
Values may be sent and summed in bfloat16 or wider, within the bound.
No kernel may reach another device: no remote copies, remote signals or barrier semaphores. Data moves between devices by JAX's collectives and lax.ppermute only.
A program may use at most 128 MiB of HBM per device.

v0:
```python
import jax
import jax.numpy as jnp
from jax import lax
from jax.sharding import Mesh
from jax.sharding import PartitionSpec as P

HEAD = 128
TP = ("tp_0", "tp_1")
GRP_SP_TP = ("grp", "sp", "tp_0", "tp_1")
EPS = 1e-06


def in_order(parts, dim):
    dims = list(parts.shape[1:])
    dims[dim] *= parts.shape[0]
    return jnp.moveaxis(parts, 0, dim).reshape(dims)


def stacked_from(x, axes, order):
    parts = x
    for k in order:
        parts = lax.all_gather(parts, axes[k])
    done = order[::-1]
    back = [done.index(k) for k in range(len(axes))]
    parts = parts.transpose(*back, *range(len(axes), parts.ndim))
    return parts.reshape(-1, *x.shape)


def whole_of(x, axes, order, dim):
    return in_order(stacked_from(x, axes, order), dim)


def sent_together(arrays, axis, dim, along):
    both = jnp.concatenate(arrays, axis=along)
    result, at, gathered = (lax.all_gather(both, axis, axis=dim, tiled=True), 0, [])
    for a in arrays:
        gathered.append(lax.slice_in_dim(result, at, at + a.shape[along], axis=along))
        at += a.shape[along]
    return tuple(gathered)


def split_up(x, dim, peers):
    dims = x.shape
    parts = x.reshape(*dims[:dim], peers, dims[dim] // peers, *dims[dim + 1 :])
    return jnp.moveaxis(parts, dim, 0)


def sum_at_owner(x, axis, dim):
    peers = lax.axis_size(axis)
    parts = lax.all_to_all(split_up(x, dim, peers), axis, 0, 0, tiled=True)
    return jnp.sum(parts.astype(jnp.float32), axis=0)


def normalize(row_block, gain_row):
    return (
        row_block
        * lax.rsqrt(jnp.mean(row_block * row_block, axis=-1, keepdims=True) + EPS)
        * gain_row
    )


def split_heads(row_block):
    return row_block.reshape(row_block.shape[0], row_block.shape[1] // HEAD, HEAD)


def body(target, source, w_query, w_key, w_value, w_out, gains):
    local_width = w_query.shape[2]
    heads_here = local_width // HEAD
    score_scale = HEAD ** (-0.5)
    depth = w_query.shape[0]
    project_shard_part = lax.all_gather(source, TP, axis=0, tiled=True)
    layer_parts = [
        jnp.stack(
            [
                jnp.dot(project_shard_part, w_key[level], preferred_element_type=jnp.float32),
                jnp.dot(project_shard_part, w_value[level], preferred_element_type=jnp.float32),
            ]
        )
        for level in range(depth)
    ]
    projected_source = jnp.stack(layer_parts).astype(jnp.bfloat16)
    stream = target.astype(jnp.float32)
    for layer_index in range(depth):
        normed = normalize(stream, gains[layer_index, 0]).astype(jnp.bfloat16)
        query_weight = w_query[layer_index]
        queries = jnp.dot(
            whole_of(normed, ("tp_0", "tp_1"), (0, 1), 0),
            query_weight,
            preferred_element_type=jnp.float32,
        ).astype(jnp.bfloat16)
        row_count = queries.shape[0]
        keys_here = projected_source[layer_index, 0]
        values_here = projected_source[layer_index, 1]
        query_heads = split_heads(queries)
        shard_part = sent_together((keys_here, values_here), "sp", 0, 1)
        row_peak = jnp.full((heads_here, row_count), -1e30, jnp.float32)
        key_heads = split_heads(shard_part[0])
        value_heads = split_heads(shard_part[1])
        scores = (
            jnp.einsum("qhd,khd->hqk", query_heads, key_heads, preferred_element_type=jnp.float32)
            * score_scale
        )
        new_peak = jnp.maximum(row_peak, jnp.max(scores, axis=2))
        weights = jnp.exp(scores - new_peak[:, :, None])
        row_total = jnp.sum(weights, axis=2)
        summed = jnp.einsum(
            "hqk,khd->hqd",
            weights.astype(jnp.bfloat16),
            value_heads,
            preferred_element_type=jnp.float32,
        )
        row_peak, row_total, summed = (new_peak, row_total, summed)
        heads_out = summed / row_total[:, :, None]
        attended = (
            jnp.transpose(heads_out, (1, 0, 2)).reshape(row_count, local_width).astype(jnp.bfloat16)
        )
        out_weight = w_out[layer_index]
        projected = sum_at_owner(
            jnp.dot(attended, out_weight, preferred_element_type=jnp.float32).astype(jnp.bfloat16),
            TP,
            0,
        )
        stream = stream + normalize(projected, gains[layer_index, 1])
    return stream.astype(jnp.bfloat16)


def solution(mesh):
    split = Mesh(
        mesh.devices.reshape(mesh.shape["grp"], mesh.shape["sp"], 8, 2),
        ("grp", "sp", "tp_0", "tp_1"),
    )
    placed = (
        P(GRP_SP_TP, None),
        P(GRP_SP_TP, None),
        P(None, None, TP),
        P(None, None, TP),
        P(None, None, TP),
        P(None, TP, None),
        P(),
    )
    return jax.shard_map(
        body, mesh=split, in_specs=placed, out_specs=P(GRP_SP_TP, None), check_vma=False
    )
```

profile of v0, /device:TPU:65, one launch (start us, length us, event | category | flops | bytes accessed | tf_op | source)
XLA Modules:
  0.0 365.9 jit_solution(10650329462650321292)
XLA Ops:
  6.6 0.7 all-gather.8.cloned.1.call-update
  7.4 85.2 %all-gather.8.cloned.1.call-done = bf16[1024,2048]{1,0:T(8,128)(2,1)} async-done(((bf16[64,2048]{1,0:T(8,128)(2,1)}), bf16[1024,2048]{1,0:T(8,128)(2,1)}) %all-gather.8.cloned.1.call-update) | async-done | bytes 4194320 | tf_op jit(solution)/shard_map/all_gather | solution.py:71
  92.6 3.8 %fusion.16 = bf16[1,1024,128]{1,2,0:T(8,128)(2,1)S(1)} fusion(bf16[1024,2048]{1,0:T(8,128)(2,1)} %all-gather.8.cloned.1.call-done, bf16[2,2048,128]{2,1,0:T(8,128)(2,1)} %param.10), kind=kOutput, calls=%fused_computation.24 | convolution fusion | flops 537001984 | bytes 4980736 | tf_op jit(solution)/shard_map/dot_general | solution.py:75
  96.4 3.8 %fusion.17 = bf16[1,1024,128]{1,2,0:T(8,128)(2,1)S(1)} fusion(bf16[1024,2048]{1,0:T(8,128)(2,1)} %all-gather.8.cloned.1.call-done, bf16[2,2048,128]{2,1,0:T(8,128)(2,1)} %param.11), kind=kOutput, calls=%fused_computation.25 | convolution fusion | flops 537001984 | bytes 4980736 | tf_op jit(solution)/shard_map/dot_general | solution.py:76
  100.4 0.8 pad_maximum_fusion
  101.3 0.1 all-gather.12.cloned.1.call-start
  101.4 3.8 %fusion.18 = bf16[1,1024,128]{1,2,0:T(8,128)(2,1)S(1)} fusion(bf16[1024,2048]{1,0:T(8,128)(2,1)} %all-gather.8.cloned.1.call-done, bf16[2,2048,128]{2,1,0:T(8,128)(2,1)S(1)} %copy-done), kind=kOutput, calls=%fused_computation.26 | convolution fusion | flops 537001984 | bytes 4980736 | tf_op jit(solution)/shard_map/dot_general | solution.py:75
  105.2 3.7 %fusion.19 = bf16[1,1024,128]{1,2,0:T(8,128)(2,1)S(1)} fusion(bf16[1024,2048]{1,0:T(8,128)(2,1)} %all-gather.8.cloned.1.call-done, bf16[2,2048,128]{2,1,0:T(8,128)(2,1)S(1)} %copy-done.1), kind=kOutput, calls=%fused_computation.27 | convolution fusion | flops 537001984 | bytes 4980736 | tf_op jit(solution)/shard_map/dot_general | solution.py:76
  109.0 0.9 pad_maximum_fusion.1
  109.9 0.1 fusion.68
  110.1 0.1 fusion.70
  110.2 19.9 %all-gather = bf16[64,2048]{1,0:T(8,128)(2,1)S(1)} all-gather(bf16[8,2048]{1,0:T(8,128)(2,1)S(1)} %fusion.70), channel_id=2, replica_groups=mesh['grp'=2,'sp'=16,'tp_0'=8,'tp_1'=2] {'tp_0'}, dimensions={0}, use_global_device_ids=true | all-gather | bytes 294912 | tf_op jit(solution)/shard_map/all_gather | solution.py:22
  130.0 7.1 %all-gather.1 = bf16[16,8,2048]{2,1,0:T(8,128)(2,1)S(1)} all-gather(bf16[8,8,2048]{2,1,0:T(8,128)(2,1)S(1)} %bitcast.78), channel_id=3, replica_groups=mesh['grp'=2,'sp'=16,'tp_0'=8,'tp_1'=2] {'tp_1'}, dimensions={0}, use_global_device_ids=true | all-gather | bytes 786432 | tf_op jit(solution)/shard_map/all_gather | solution.py:22
  137.1 71.2 %all-gather.10.cloned.1.call-done = bf16[16384,256]{0,1:T(8,128)(2,1)} async-done(((bf16[1024,256]{0,1:T(8,128)(2,1)}), bf16[16384,256]{0,1:T(8,128)(2,1)}) %all-gather.10.cloned.1.call-update) | async-done | bytes 8388624 | tf_op jit(solution)/shard_map/all_gather | solution.py:35
  208.4 7.0 %fusion.74 = (f32[128]{0:T(128)S(1)}, f32[128,16384]{1,0:T(8,128)}) fusion(bf16[16384,256]{0,1:T(8,128)(2,1)} %all-gather.10.cloned.1.call-done, bf16[128,2048]{1,0:T(8,128)(2,1)S(1)} %bitcast.76, bf16[2,2048,128]{2,1,0:T(8,128)(2,1)S(1)} %copy-done.3), kind=kOutput, calls=%fused_computation.80 | convolution fusion | flops 608190336 | bytes 13632000 | tf_op jit(solution)/shard_map/qhd,khd->hqk/dot_general | solution.py:100
  215.3 4.7 %fusion = f32[128]{0:T(128)S(1)} fusion(f32[128,16384]{1,0:T(8,128)} %get-tuple-element.14, f32[128]{0:T(128)S(1)} %broadcast_maximum_fusion.1), kind=kLoop, calls=%fused_computation.4 | loop fusion | flops 4194176 | bytes 8389632 | tf_op jit(solution)/shard_map/reduce_sum | solution.py:105
  220.0 6.4 %fusion.14 = bf16[16,8,2048]{2,1,0:T(8,128)(2,1)S(1)} fusion(bf16[16384,256]{0,1:T(8,128)(2,1)} %all-gather.10.cloned.1.call-done, f32[128,16384]{1,0:T(8,128)} %get-tuple-element.14, f32[128]{0:T(128)S(1)} %broadcast_maximum_fusion.1, bf16[2,128,2048]{2,1,0:T(8,128)(2,1)S(1)} %copy-done.2, f32[128]{0:T(128)S(1)} %fusion), kind=kOutput, calls=%fused_computation.18 | convolution fusion | flops 608468992 | bytes 13632512 | tf_op jit(solution)/shard_map/dot_general | solution.py:119
  226.4 24.5 %all_to_all.10 = bf16[16,8,2048]{2,1,0:T(8,128)(2,1)S(1)} all-to-all(bf16[16,8,2048]{2,1,0:T(8,128)(2,1)S(1)} %fusion.14), channel_id=1, replica_groups=mesh['grp'=2,'sp'=16,'tp_0'=8,'tp_1'=2] {'tp_0','tp_1'}, dimensions={0} | all-to-all | bytes 1048576 | tf_op jit(solution)/shard_map/all_to_all | solution.py:50
  251.0 0.1 convert_reduce_fusion.1
  251.0 0.1 multiply_reduce_fusion.2
  251.2 0.2 multiply_reduce_fusion.1
  251.4 0.1 multiply_convert_fusion
  251.5 21.5 %all-gather.2 = bf16[64,2048]{1,0:T(8,128)(2,1)S(1)} all-gather(bf16[8,2048]{1,0:T(8,128)(2,1)S(1)} %multiply_convert_fusion), channel_id=4, replica_groups=mesh['grp'=2,'sp'=16,'tp_0'=8,'tp_1'=2] {'tp_0'}, dimensions={0}, use_global_device_ids=true | all-gather | bytes 294912 | tf_op jit(solution)/shard_map/all_gather | solution.py:22
  272.9 4.2 %all-gather.3 = bf16[16,8,2048]{2,1,0:T(8,128)(2,1)S(1)} all-gather(bf16[8,8,2048]{2,1,0:T(8,128)(2,1)S(1)} %bitcast.79), channel_id=5, replica_groups=mesh['grp'=2,'sp'=16,'tp_0'=8,'tp_1'=2] {'tp_1'}, dimensions={0}, use_global_device_ids=true | all-gather | bytes 786432 | tf_op jit(solution)/shard_map/all_gather | solution.py:22
  277.2 38.7 %all-gather.12.cloned.1.call-done = bf16[16384,256]{0,1:T(8,128)(2,1)} async-done(((bf16[1024,256]{0,1:T(8,128)(2,1)}), bf16[16384,256]{0,1:T(8,128)(2,1)}) %all-gather.12.cloned.1.call-update) | async-done | bytes 8388624 | tf_op jit(solution)/shard_map/all_gather | solution.py:35
  315.9 6.9 %fusion.77 = (f32[128]{0:T(128)S(1)}, f32[128,16384]{1,0:T(8,128)}) fusion(bf16[16384,256]{0,1:T(8,128)(2,1)} %all-gather.12.cloned.1.call-done, bf16[128,2048]{1,0:T(8,128)(2,1)S(1)} %bitcast.77, bf16[2,2048,128]{2,1,0:T(8,128)(2,1)S(1)} %copy-done.3), kind=kOutput, calls=%fused_computation.81 | convolution fusion | flops 608190336 | bytes 13632000 | tf_op jit(solution)/shard_map/qhd,khd->hqk/dot_general | solution.py:100
  322.8 4.7 %fusion.2 = f32[128]{0:T(128)S(1)} fusion(f32[128,16384]{1,0:T(8,128)} %get-tuple-element.16, f32[128]{0:T(128)S(1)} %broadcast_maximum_fusion), kind=kLoop, calls=%fused_computation.6 | loop fusion | flops 4194176 | bytes 8389632 | tf_op jit(solution)/shard_map/reduce_sum | solution.py:105
  327.5 6.4 %fusion.15 = bf16[16,8,2048]{2,1,0:T(8,128)(2,1)S(1)} fusion(bf16[16384,256]{0,1:T(8,128)(2,1)} %all-gather.12.cloned.1.call-done, f32[128,16384]{1,0:T(8,128)} %get-tuple-element.16, f32[128]{0:T(128)S(1)} %broadcast_maximum_fusion, bf16[2,128,2048]{2,1,0:T(8,128)(2,1)S(1)} %copy-done.2, f32[128]{0:T(128)S(1)} %fusion.2), kind=kOutput, calls=%fused_computation.19 | convolution fusion | flops 608468992 | bytes 13632512 | tf_op jit(solution)/shard_map/dot_general | solution.py:119
  333.9 24.6 %all_to_all.11 = bf16[16,8,2048]{2,1,0:T(8,128)(2,1)S(1)} all-to-all(bf16[16,8,2048]{2,1,0:T(8,128)(2,1)S(1)} %fusion.15), channel_id=1, replica_groups=mesh['grp'=2,'sp'=16,'tp_0'=8,'tp_1'=2] {'tp_0','tp_1'}, dimensions={0} | all-to-all | bytes 1048576 | tf_op jit(solution)/shard_map/all_to_all | solution.py:50
  358.4 0.1 convert_reduce_fusion
  358.5 0.1 multiply_reduce_fusion
  358.6 0.7 add_convert_fusion
  (29 shorter events, 0.5 us)
Async XLA Ops:
  6.5 94.8 %copy-start = (bf16[2,2048,128]{2,1,0:T(8,128)(2,1)S(1)}, bf16[2,2048,128]{2,1,0:T(8,128)(2,1)}, u32[]{:S(2)}) copy-start(bf16[2,2048,128]{2,1,0:T(8,128)(2,1)} %param.10) | copy-start | bytes 3145732
  6.5 86.1 %all-gather.8.cloned.1.call-start = ((), (), s32[]{:S(2)}) async-start(), calls=%async_computation.2 | async-start | bytes 4456448 | tf_op jit(solution)/shard_map/all_gather | solution.py:71
  7.3 97.8 %copy-start.1 = (bf16[2,2048,128]{2,1,0:T(8,128)(2,1)S(1)}, bf16[2,2048,128]{2,1,0:T(8,128)(2,1)}, u32[]{:S(2)}) copy-start(bf16[2,2048,128]{2,1,0:T(8,128)(2,1)} %param.11) | copy-start | bytes 3145732
  7.3 201.0 %all-gather.10.cloned.1.call-start = ((), (), s32[]{:S(2)}) async-start(), calls=%async_computation.3 | async-start | bytes 8912896 | tf_op jit(solution)/shard_map/all_gather | solution.py:35
  100.3 9.6 %copy-start.4 = (bf16[8,2048]{1,0:T(8,128)(2,1)S(1)}, bf16[8,2048]{1,0:T(8,128)(2,1)}, u32[]{:S(2)}) copy-start(bf16[8,2048]{1,0:T(8,128)(2,1)} %param.7) | copy-start | bytes 98308
  100.3 9.7 %copy-start.5 = (f32[2,2,2048]{2,1,0:T(2,128)S(1)}, f32[2,2,2048]{2,1,0:T(2,128)}, u32[]{:S(2)}) copy-start(f32[2,2,2048]{2,1,0:T(2,128)} %param.13) | copy-start | bytes 98308
  101.2 107.1 %copy-start.3 = (bf16[2,2048,128]{2,1,0:T(8,128)(2,1)S(1)}, bf16[2,2048,128]{2,1,0:T(8,128)(2,1)}, u32[]{:S(2)}) copy-start(bf16[2,2048,128]{2,1,0:T(8,128)(2,1)} %param.9) | copy-start | bytes 3145732
  101.3 214.7 %all-gather.12.cloned.1.call-start = ((), (), s32[]{:S(2)}) async-start(), calls=%async_computation.4 | async-start | bytes 8912896 | tf_op jit(solution)/shard_map/all_gather | solution.py:35
  208.4 11.7 %copy-start.2 = (bf16[2,128,2048]{2,1,0:T(8,128)(2,1)S(1)}, bf16[2,128,2048]{2,1,0:T(8,128)(2,1)}, u32[]{:S(2)}) copy-start(bf16[2,128,2048]{2,1,0:T(8,128)(2,1)} %param.12) | copy-start | bytes 3145732
Sparse Core Ops, SparseCore 0:
  9.5 83.0 all-gather.7
  101.4 106.9 all-gather.9
  210.5 105.4 all-gather.11
where the time goes:
time: 366 us
  waiting for transfers between devices  196 us (54%)
  blocking collectives  102 us (28%)
  matrix products  41.7 us (11%)
  between operations  13.3 us (4%)
  other arithmetic  12.8 us (3%)
    all_gather x2, waiting for transfers between devices, sent_together(): lax.all_gather(both, axis, axis=dim, tiled=True)  110 us
    all_gather x1, waiting for transfers between devices, body(): project_shard_part = lax.all_gather(source, TP, axis=0, tiled=True)  85.2 us
    all_gather x4, blocking collectives, stacked_from(): parts = lax.all_gather(parts, axes[k])  52.6 us
    all_to_all x2, blocking collectives, sum_at_owner(): parts = lax.all_to_all(split_up(x, dim, peers), axis, 0, 0, tiled=True)  49.1 us
    dot_general x2, matrix products, body(): jnp.einsum('qhd,khd->hqk', query_heads, key_heads, preferred_element_type...  13.9 us
    dot_general x2, matrix products, body(): jnp.dot(attended, out_weight, preferred_element_type=jnp.float32)  12.7 us
    reduce_sum x2, other arithmetic, body(): row_total = jnp.sum(weights, axis=2)  9.35 us
    dot_general x2, matrix products, body(): jnp.dot(project_shard_part, w_key[level], preferred_element_type=jnp.floa...  7.6 us
  transfers between devices with their start and end apart: 3, of which 3 were waited for; matrix products, arithmetic and copies ran while one was open for 7% of the time, Pallas kernels for 0%

commit v1 on v0

--- a/solution.py
+++ b/solution.py
@@ -68,7 +68,10 @@
     heads_here = local_width // HEAD
     score_scale = HEAD ** (-0.5)
     depth = w_query.shape[0]
-    project_shard_part = lax.all_gather(source, TP, axis=0, tiled=True)
+    size = lax.axis_size(TP)
+    shards = jnp.stack([source for _ in range(size)])
+    shards = lax.all_to_all(shards, TP, split_axis=0, concat_axis=0)
+    project_shard_part = jnp.concatenate(shards, axis=0)
     layer_parts = [
         jnp.stack(
             [

time: 366 us -> 413 us (1.13)
  blocking collectives: 102 us -> 240 us
  waiting for transfers between devices: 196 us -> 106 us
  matrix products: 41.7 us -> 37.1 us
    all_to_all x0 -> x1, blocking collectives: none -> 140 us  [body(): shards = lax.all_to_all(shards, TP, split_axis=0, concat_axis=0)]
    all_gather x1 -> x0, waiting for transfers between devices: 85.2 us -> none  [body(): project_shard_part = lax.all_gather(source, TP, axis=0, tiled=True)]
  transfers between devices with their start and end apart: 3 -> 2, of which waited for: 3 -> 2; matrix products, arithmetic and copies ran while one was open for 7% -> 7% of each run, Pallas kernels for 0% -> 0%
where the time goes in v1:
time: 413 us; the launch traced here: 412 us
  blocking collectives  240 us (58%)
  waiting for transfers between devices  106 us (26%)
  matrix products  37.1 us (9%)
  between operations  13.6 us (3%)
  other arithmetic  12.8 us (3%)
    all_to_all x1, blocking collectives, body(): shards = lax.all_to_all(shards, TP, split_axis=0, concat_axis=0)  140 us
    all_gather x2, waiting for transfers between devices, sent_together(): lax.all_gather(both, axis, axis=dim, tiled=True)  106 us
    all_gather x4, blocking collectives, stacked_from(): parts = lax.all_gather(parts, axes[k])  51.2 us
    all_to_all x2, blocking collectives, sum_at_owner(): parts = lax.all_to_all(split_up(x, dim, peers), axis, 0, 0, tiled=True)  49.1 us
    dot_general x2, matrix products, body(): jnp.einsum('qhd,khd->hqk', query_heads, key_heads, preferred_element_type...  13.9 us
    dot_general x2, matrix products, body(): jnp.dot(attended, out_weight, preferred_element_type=jnp.float32)  12.7 us
    reduce_sum x2, other arithmetic, body(): row_total = jnp.sum(weights, axis=2)  9.35 us
  transfers between devices with their start and end apart: 2, of which 2 were waited for; matrix products, arithmetic and copies ran while one was open for 7% of the time, Pallas kernels for 0%

profile of v1, /device:TPU:65, one launch (start us, length us, event | category | flops | bytes accessed | tf_op | source)
XLA Modules:
  0.0 412.2 jit_solution(8094688842044721145)
XLA Ops:
  6.6 1.6 stack.53
  8.2 139.8 %all_to_all.15 = bf16[16,64,2048]{2,1,0:T(8,128)(2,1)S(1)} all-to-all(bf16[16,64,2048]{2,1,0:T(8,128)(2,1)S(1)} %stack.53), channel_id=1, replica_groups=mesh['grp'=2,'sp'=16,'tp_0'=8,'tp_1'=2] {'tp_0','tp_1'}, dimensions={0} | all-to-all | bytes 8388608 | tf_op jit(solution)/shard_map/all_to_all | solution.py:73
  147.9 1.5 fusion.16
  149.5 0.4 copy-done
  149.9 1.5 fusion.17
  151.5 0.8 pad_maximum_fusion
  152.5 3.8 fusion.18
  156.3 3.7 fusion.19
  160.1 0.9 pad_maximum_fusion.1
  161.0 0.1 fusion.68
  161.2 0.1 fusion.70
  161.3 20.4 %all-gather = bf16[64,2048]{1,0:T(8,128)(2,1)S(1)} all-gather(bf16[8,2048]{1,0:T(8,128)(2,1)S(1)} %fusion.70), channel_id=2, replica_groups=mesh['grp'=2,'sp'=16,'tp_0'=8,'tp_1'=2] {'tp_0'}, dimensions={0}, use_global_device_ids=true | all-gather | bytes 294912 | tf_op jit(solution)/shard_map/all_gather | solution.py:22
  181.7 5.2 %all-gather.1 = bf16[16,8,2048]{2,1,0:T(8,128)(2,1)S(1)} all-gather(bf16[8,8,2048]{2,1,0:T(8,128)(2,1)S(1)} %bitcast.83), channel_id=3, replica_groups=mesh['grp'=2,'sp'=16,'tp_0'=8,'tp_1'=2] {'tp_1'}, dimensions={0}, use_global_device_ids=true | all-gather | bytes 786432 | tf_op jit(solution)/shard_map/all_gather | solution.py:22
  187.0 67.4 %all-gather.7.cloned.1.call-done = bf16[16384,256]{0,1:T(8,128)(2,1)} async-done(((bf16[1024,256]{0,1:T(8,128)(2,1)}), bf16[16384,256]{0,1:T(8,128)(2,1)}) %all-gather.7.cloned.1.call-update) | async-done | bytes 8388624 | tf_op jit(solution)/shard_map/all_gather | solution.py:35
  254.4 7.0 %fusion.74 = (f32[128]{0:T(128)S(1)}, f32[128,16384]{1,0:T(8,128)}) fusion(bf16[16384,256]{0,1:T(8,128)(2,1)} %all-gather.7.cloned.1.call-done, bf16[128,2048]{1,0:T(8,128)(2,1)S(1)} %bitcast.81, bf16[2,2048,128]{2,1,0:T(8,128)(2,1)S(1)} %copy-done.4), kind=kOutput, calls=%fused_computation.80 | convolution fusion | flops 608190336 | bytes 13632000 | tf_op jit(solution)/shard_map/qhd,khd->hqk/dot_general | solution.py:103
  261.4 4.7 %fusion = f32[128]{0:T(128)S(1)} fusion(f32[128,16384]{1,0:T(8,128)} %get-tuple-element.14, f32[128]{0:T(128)S(1)} %broadcast_maximum_fusion.1), kind=kLoop, calls=%fused_computation.4 | loop fusion | flops 4194176 | bytes 8389632 | tf_op jit(solution)/shard_map/reduce_sum | solution.py:108
  266.0 6.4 %fusion.14 = bf16[16,8,2048]{2,1,0:T(8,128)(2,1)S(1)} fusion(bf16[16384,256]{0,1:T(8,128)(2,1)} %all-gather.7.cloned.1.call-done, f32[128,16384]{1,0:T(8,128)} %get-tuple-element.14, f32[128]{0:T(128)S(1)} %broadcast_maximum_fusion.1, bf16[2,128,2048]{2,1,0:T(8,128)(2,1)S(1)} %copy-done.3, f32[128]{0:T(128)S(1)} %fusion), kind=kOutput, calls=%fused_computation.18 | convolution fusion | flops 608468992 | bytes 13632512 | tf_op jit(solution)/shard_map/dot_general | solution.py:122
  272.4 24.6 %all_to_all.16 = bf16[16,8,2048]{2,1,0:T(8,128)(2,1)S(1)} all-to-all(bf16[16,8,2048]{2,1,0:T(8,128)(2,1)S(1)} %fusion.14), channel_id=1, replica_groups=mesh['grp'=2,'sp'=16,'tp_0'=8,'tp_1'=2] {'tp_0','tp_1'}, dimensions={0} | all-to-all | bytes 1048576 | tf_op jit(solution)/shard_map/all_to_all | solution.py:50
  297.0 0.1 convert_reduce_fusion.1
  297.0 0.1 multiply_reduce_fusion.2
  297.2 0.2 multiply_reduce_fusion.1
  297.4 0.1 multiply_convert_fusion
  297.5 21.3 %all-gather.2 = bf16[64,2048]{1,0:T(8,128)(2,1)S(1)} all-gather(bf16[8,2048]{1,0:T(8,128)(2,1)S(1)} %multiply_convert_fusion), channel_id=4, replica_groups=mesh['grp'=2,'sp'=16,'tp_0'=8,'tp_1'=2] {'tp_0'}, dimensions={0}, use_global_device_ids=true | all-gather | bytes 294912 | tf_op jit(solution)/shard_map/all_gather | solution.py:22
  318.8 4.2 %all-gather.3 = bf16[16,8,2048]{2,1,0:T(8,128)(2,1)S(1)} all-gather(bf16[8,8,2048]{2,1,0:T(8,128)(2,1)S(1)} %bitcast.84), channel_id=5, replica_groups=mesh['grp'=2,'sp'=16,'tp_0'=8,'tp_1'=2] {'tp_1'}, dimensions={0}, use_global_device_ids=true | all-gather | bytes 786432 | tf_op jit(solution)/shard_map/all_gather | solution.py:22
  323.0 38.9 %all-gather.9.cloned.1.call-done = bf16[16384,256]{0,1:T(8,128)(2,1)} async-done(((bf16[1024,256]{0,1:T(8,128)(2,1)}), bf16[16384,256]{0,1:T(8,128)(2,1)}) %all-gather.9.cloned.1.call-update) | async-done | bytes 8388624 | tf_op jit(solution)/shard_map/all_gather | solution.py:35
  361.9 6.9 %fusion.77 = (f32[128]{0:T(128)S(1)}, f32[128,16384]{1,0:T(8,128)}) fusion(bf16[16384,256]{0,1:T(8,128)(2,1)} %all-gather.9.cloned.1.call-done, bf16[128,2048]{1,0:T(8,128)(2,1)S(1)} %bitcast.82, bf16[2,2048,128]{2,1,0:T(8,128)(2,1)S(1)} %copy-done.4), kind=kOutput, calls=%fused_computation.81 | convolution fusion | flops 608190336 | bytes 13632000 | tf_op jit(solution)/shard_map/qhd,khd->hqk/dot_general | solution.py:103
  368.8 4.7 %fusion.2 = f32[128]{0:T(128)S(1)} fusion(f32[128,16384]{1,0:T(8,128)} %get-tuple-element.16, f32[128]{0:T(128)S(1)} %broadcast_maximum_fusion), kind=kLoop, calls=%fused_computation.6 | loop fusion | flops 4194176 | bytes 8389632 | tf_op jit(solution)/shard_map/reduce_sum | solution.py:108
  373.5 6.4 %fusion.15 = bf16[16,8,2048]{2,1,0:T(8,128)(2,1)S(1)} fusion(bf16[16384,256]{0,1:T(8,128)(2,1)} %all-gather.9.cloned.1.call-done, f32[128,16384]{1,0:T(8,128)} %get-tuple-element.16, f32[128]{0:T(128)S(1)} %broadcast_maximum_fusion, bf16[2,128,2048]{2,1,0:T(8,128)(2,1)S(1)} %copy-done.3, f32[128]{0:T(128)S(1)} %fusion.2), kind=kOutput, calls=%fused_computation.19 | convolution fusion | flops 608468992 | bytes 13632512 | tf_op jit(solution)/shard_map/dot_general | solution.py:122
  379.9 24.6 %all_to_all.17 = bf16[16,8,2048]{2,1,0:T(8,128)(2,1)S(1)} all-to-all(bf16[16,8,2048]{2,1,0:T(8,128)(2,1)S(1)} %fusion.15), channel_id=1, replica_groups=mesh['grp'=2,'sp'=16,'tp_0'=8,'tp_1'=2] {'tp_0','tp_1'}, dimensions={0} | all-to-all | bytes 1048576 | tf_op jit(solution)/shard_map/all_to_all | solution.py:50
  404.4 0.1 convert_reduce_fusion
  404.5 0.1 multiply_reduce_fusion
  404.6 0.7 add_convert_fusion
  (30 shorter events, 0.5 us)
Async XLA Ops:
  6.5 141.4 %copy-start.1 = (bf16[2,2048,128]{2,1,0:T(8,128)(2,1)S(1)}, bf16[2,2048,128]{2,1,0:T(8,128)(2,1)}, u32[]{:S(2)}) copy-start(bf16[2,2048,128]{2,1,0:T(8,128)(2,1)} %param.10) | copy-start | bytes 3145732
  6.5 143.3 %copy-start.2 = (bf16[2,2048,128]{2,1,0:T(8,128)(2,1)S(1)}, bf16[2,2048,128]{2,1,0:T(8,128)(2,1)}, u32[]{:S(2)}) copy-start(bf16[2,2048,128]{2,1,0:T(8,128)(2,1)} %param.11) | copy-start | bytes 3145732
  6.6 247.8 %all-gather.7.cloned.1.call-start = ((), (), s32[]{:S(2)}) async-start(), calls=%async_computation.3 | async-start | bytes 8912896 | tf_op jit(solution)/shard_map/all_gather | solution.py:35
  147.9 1.9 copy-start
  151.4 9.6 %copy-start.5 = (bf16[8,2048]{1,0:T(8,128)(2,1)S(1)}, bf16[8,2048]{1,0:T(8,128)(2,1)}, u32[]{:S(2)}) copy-start(bf16[8,2048]{1,0:T(8,128)(2,1)} %param.7) | copy-start | bytes 98308
  151.5 9.7 %copy-start.6 = (f32[2,2,2048]{2,1,0:T(2,128)S(1)}, f32[2,2,2048]{2,1,0:T(2,128)}, u32[]{:S(2)}) copy-start(f32[2,2,2048]{2,1,0:T(2,128)} %param.13) | copy-start | bytes 98308
  152.3 102.0 %copy-start.4 = (bf16[2,2048,128]{2,1,0:T(8,128)(2,1)S(1)}, bf16[2,2048,128]{2,1,0:T(8,128)(2,1)}, u32[]{:S(2)}) copy-start(bf16[2,2048,128]{2,1,0:T(8,128)(2,1)} %param.9) | copy-start | bytes 3145732
  152.4 209.5 %all-gather.9.cloned.1.call-start = ((), (), s32[]{:S(2)}) async-start(), calls=%async_computation.4 | async-start | bytes 8912896 | tf_op jit(solution)/shard_map/all_gather | solution.py:35
  254.4 11.7 %copy-start.3 = (bf16[2,128,2048]{2,1,0:T(8,128)(2,1)S(1)}, bf16[2,128,2048]{2,1,0:T(8,128)(2,1)}, u32[]{:S(2)}) copy-start(bf16[2,128,2048]{2,1,0:T(8,128)(2,1)} %param.12) | copy-start | bytes 3145732
Sparse Core Ops, SparseCore 0:
  152.5 101.7 all-gather.6
  256.5 105.4 all-gather.8
